TPU v7x, 128 devices: a whole 4x4x4 slice. The times are simulated.
128 devices in a mesh: ep: 64 (over z, y, x), tp: 2 (over core).
Axes of the slice: x: 4, y: 4, z: 4, core: 2. Of those that a mesh axis runs over, the one named last changes fastest.
Arguments:
- residual: bfloat16 [1024, 4096], P(('ep', 'tp')), may hold values from -6 to 6
- lengths: int32 [1024], P(('ep', 'tp')), may hold values from 128 to 1024
- latent_cache: bfloat16 [1024, 1024, 512], P(('ep', 'tp'))
- rope_cache: bfloat16 [1024, 1024, 64], P(('ep', 'tp')), may hold values from -6 to 6
- route_ids: int32 [1024, 2], P(('ep', 'tp')), may hold values from 0 to 7, all different within a row; in each aligned block of 8 rows (0 to 7, 8 to 15, ...) at most 3 rows name the same one
- route_scores: bfloat16 [1024, 2], P(('ep', 'tp')), may hold values from -6 to 6
- norm_first: float32 [4096], replicated, may hold values from 0.1 to 1.9
- norm_second: float32 [4096], replicated, may hold values from 0.1 to 1.9
- query_gain: float32 [1024], replicated, may hold values from 0.1 to 1.9
- latent_gain: float32 [512], replicated, may hold values from 0.1 to 1.9
- query_down: bfloat16 [4096, 1024], P(('ep', 'tp')), may hold values from -0.09375 to 0.09375
- latent_down: bfloat16 [4096, 512], P(('ep', 'tp')), may hold values from -0.09375 to 0.09375
- rope_down: bfloat16 [4096, 64], replicated, may hold values from -0.09375 to 0.09375
- query_latent: bfloat16 [1024, 16384], P(None, ('ep', 'tp')), may hold values from -0.1875 to 0.1875
- query_rope: bfloat16 [1024, 2048], P(None, ('ep', 'tp')), may hold values from -0.1875 to 0.1875
- value_up: bfloat16 [512, 32, 128], replicated, may hold values from -1 to 1
- output_weight: bfloat16 [4096, 4096], P(None, ('ep', 'tp')), may hold values from -0.09375 to 0.09375
- expert_gate: bfloat16 [4096, 57344], P(None, ('ep', 'tp')), may hold values from -0.09375 to 0.09375
- expert_up: bfloat16 [4096, 57344], P(None, ('ep', 'tp')), may hold values from -0.09375 to 0.09375
- expert_down: bfloat16 [57344, 4096], P(('ep', 'tp')), may hold values from -0.125 to 0.125
Outputs:
- layer_out: bfloat16 [1024, 4096], P(('ep', 'tp'))
- new_latent: bfloat16 [1024, 512], P(('ep', 'tp'))
- new_rope: bfloat16 [1024, 64], P(('ep', 'tp'))
Inputs may be any that keep to these rules, and one draw needn't show every extreme that they name: `route_ids`: each row names 2 different experts. Within the rows of one device (aligned blocks of 8 rows) no expert is named more than 3 times; in every draw some expert is named exactly 3 times in some blocks. `lengths`: A sequence's cached positions are 0 to its length - 1; the new token stands at position length.
All inputs are finite; a program needn't handle non-finite values.
Results may differ from a plain program's by a relative error of at most 0.014.
The roundings to bfloat16 on the way count: a program that leaves them out, or rounds other values in their place, can miss the bound.
Values may be sent and summed in bfloat16 or wider, within the bound.
A program may use at most 128 MiB of HBM per device.

v0:
```python
import jax
import jax.numpy as jnp
from jax import lax
from jax.sharding import Mesh
from jax.sharding import PartitionSpec as P

ROPE = 64
NOPE = 128
EXPERTS = 8
TOP = 2
CAP = 3
EP_TP = ("ep_0", "ep_1", "ep_2", "tp")
epsilon = 1e-06
rope_base = 10000.0


def cut_along(shard, dim, peers):
    before, after = (shard.shape[:dim], shard.shape[dim + 1 :])
    return jnp.moveaxis(shard.reshape(*before, peers, -1, *after), dim, 0)


def sent_and_summed(shard, axis, dim):
    parts = cut_along(shard, dim, lax.axis_size(axis))
    arrived = lax.all_to_all(parts, axis, split_axis=0, concat_axis=0, tiled=True)
    return arrived.sum(axis=0)


def sum_by_axis(shard, axes, dim):
    far, near = axes
    parts = cut_along(shard, dim, lax.axis_size(far))
    nearer = sent_and_summed(parts, near, dim + 1)
    arrived = lax.all_to_all(nearer, far, split_axis=0, concat_axis=0, tiled=True)
    return arrived.sum(axis=0)


def sent_to_all(shard, axis):
    peers = lax.axis_size(axis)
    return lax.all_to_all(
        jnp.broadcast_to(shard[None], (peers, *shard.shape)), axis, 0, 0, tiled=True
    )


def in_order(parts, dim):
    shape = list(parts.shape[1:])
    shape[dim] *= parts.shape[0]
    return jnp.moveaxis(parts, 0, dim).reshape(shape)


def gathered_by_axis(shard, axes, dim):
    far, near = axes
    parts = sent_to_all(sent_to_all(shard, far), near)
    return in_order(parts.swapaxes(0, 1).reshape(-1, *shard.shape), dim)


def normalize(values_in, gain_row):
    return (
        values_in
        * lax.rsqrt(jnp.mean(values_in * values_in, axis=-1, keepdims=True) + epsilon)
        * gain_row
    )


def rotate(values_in, turns):
    half_width = values_in.shape[-1] // 2
    front_half = values_in[..., :half_width]
    back_half = values_in[..., half_width:]
    cosine = jnp.cos(turns)
    sine_part = jnp.sin(turns)
    return jnp.concatenate(
        [front_half * cosine - back_half * sine_part, front_half * sine_part + back_half * cosine],
        axis=-1,
    )


def rotary_angles(positions, rotary_width):
    inverse = rope_base ** (-jnp.arange(0, rotary_width, 2, dtype=jnp.float32) / rotary_width)
    return positions.astype(jnp.float32)[:, None] * inverse[None, :]


def slot_tables(route_block):
    experts = jnp.arange(EXPERTS, dtype=jnp.int32)
    onehot = (route_block[..., None] == experts).astype(jnp.int32)
    earlier = jnp.cumsum(onehot, axis=-2) - onehot
    slot_rank = jnp.sum(earlier * onehot, axis=-1)
    places = jnp.arange(CAP, dtype=jnp.int32)
    return onehot[..., None] * (slot_rank[..., None, None] == places).astype(jnp.int32)


def owner_table(sequences):
    assign = sequences * TOP
    return (
        jnp.arange(assign, dtype=jnp.int32)[None, :] // TOP
        == jnp.arange(sequences, dtype=jnp.int32)[:, None]
    ).astype(jnp.float32)


def expert_rows(row_block, expert_gate, expert_up, expert_down):
    gate_part = jnp.dot(row_block, expert_gate, preferred_element_type=jnp.float32)
    up_part = jnp.dot(row_block, expert_up, preferred_element_type=jnp.float32)
    hidden = (jax.nn.silu(gate_part) * up_part).astype(jnp.bfloat16)
    return jnp.dot(hidden, expert_down, preferred_element_type=jnp.float32)


def attend_local(
    query_latents, query_rotary, latent_cache, rope_cache, new_latent, new_rope, lengths
):
    score_scale = (NOPE + ROPE) ** (-0.5)
    cache_scores = (
        jnp.einsum("shl,spl->shp", query_latents, latent_cache, preferred_element_type=jnp.float32)
        + jnp.einsum("shr,spr->shp", query_rotary, rope_cache, preferred_element_type=jnp.float32)
    ) * score_scale
    new_scores = (
        jnp.einsum("shl,sl->sh", query_latents, new_latent, preferred_element_type=jnp.float32)
        + jnp.einsum("shr,sr->sh", query_rotary, new_rope, preferred_element_type=jnp.float32)
    ) * score_scale
    visible = jnp.arange(latent_cache.shape[1], dtype=jnp.int32)[None, :] < lengths[:, None]
    cache_scores = jnp.where(visible[:, None, :], cache_scores, -jnp.inf)
    row_top = jnp.maximum(jnp.max(cache_scores, axis=-1), new_scores)
    cache_terms = jnp.exp(cache_scores - row_top[..., None])
    new_term = jnp.exp(new_scores - row_top)
    denominator = jnp.sum(cache_terms, axis=-1) + new_term
    cache_probs = (cache_terms / denominator[..., None]).astype(jnp.bfloat16)
    new_probs = (new_term / denominator).astype(jnp.bfloat16)
    mixture = jnp.einsum(
        "shp,spl->shl", cache_probs, latent_cache, preferred_element_type=jnp.float32
    )
    mixture = (
        mixture
        + new_probs.astype(jnp.float32)[..., None] * new_latent.astype(jnp.float32)[:, None, :]
    )
    return mixture.astype(jnp.bfloat16)


def local(
    residual,
    lengths,
    latent_cache,
    rope_cache,
    route_ids,
    route_scores,
    norm_first,
    norm_second,
    query_gain,
    latent_gain,
    query_down,
    latent_down,
    rope_down,
    query_latent,
    query_rope,
    value_up,
    output_weight,
    expert_gate,
    expert_up,
    expert_down,
):
    sequences = residual.shape[0]
    model_width = residual.shape[1]
    devices = lax.axis_size(EP_TP)
    stream = residual.astype(jnp.float32)
    normed = normalize(stream, norm_first).astype(jnp.bfloat16)
    slices = lax.all_to_all(normed, EP_TP, split_axis=1, concat_axis=0, tiled=True)
    query_width = query_down.shape[1]
    lowered = sum_by_axis(
        jnp.concatenate(
            [
                jnp.dot(slices, query_down, preferred_element_type=jnp.float32),
                jnp.dot(slices, latent_down, preferred_element_type=jnp.float32),
            ],
            axis=1,
        ),
        (("ep_0", "ep_1", "ep_2"), "tp"),
        0,
    )
    query_small = normalize(lowered[:, :query_width], query_gain).astype(jnp.bfloat16)
    new_latent = normalize(lowered[:, query_width:], latent_gain).astype(jnp.bfloat16)
    turns = rotary_angles(lengths, rope_down.shape[1])
    new_rope = rotate(jnp.dot(normed, rope_down, preferred_element_type=jnp.float32), turns).astype(
        jnp.bfloat16
    )
    latent_columns = query_latent.shape[1]
    shard_rows = gathered_by_axis(query_small, (("ep_0", "ep_1", "ep_2"), "tp"), 0)
    columns = jnp.concatenate(
        [
            jnp.dot(shard_rows, query_latent, preferred_element_type=jnp.float32),
            jnp.dot(shard_rows, query_rope, preferred_element_type=jnp.float32),
        ],
        axis=1,
    ).astype(jnp.bfloat16)
    at_home = lax.all_to_all(columns, EP_TP, split_axis=0, concat_axis=1, tiled=True)
    at_home = at_home.reshape(sequences, devices, columns.shape[1])
    head_count = value_up.shape[1]
    query_latents = at_home[:, :, :latent_columns].reshape(sequences, head_count, -1)
    query_pe = at_home[:, :, latent_columns:].reshape(sequences, head_count, -1)
    query_rotary = rotate(query_pe.astype(jnp.float32), turns[:, None, :]).astype(jnp.bfloat16)
    mixture = attend_local(
        query_latents, query_rotary, latent_cache, rope_cache, new_latent, new_rope, lengths
    )
    values = jnp.einsum("shl,lhv->shv", mixture, value_up, preferred_element_type=jnp.float32)
    values = values.astype(jnp.bfloat16).reshape(sequences, -1)
    output_cols = jnp.dot(
        lax.all_gather(values, EP_TP, axis=0, tiled=True),
        output_weight,
        preferred_element_type=jnp.float32,
    ).astype(jnp.bfloat16)
    attended = lax.all_to_all(output_cols, EP_TP, split_axis=0, concat_axis=1, tiled=True)
    after_attention = stream + attended.astype(jnp.float32)
    second = normalize(after_attention, norm_second).astype(jnp.bfloat16)
    owners = owner_table(sequences)
    assign = sequences * TOP
    group_size = devices // EXPERTS
    weights = jax.nn.softmax(route_scores.astype(jnp.float32), axis=-1)
    matches = slot_tables(route_ids.reshape(1, assign))[0].astype(jnp.float32)
    picker = jnp.einsum("aec,sa->ecs", matches, owners).astype(jnp.bfloat16)
    outbound = jnp.einsum("ecs,sd->ecd", picker, second, preferred_element_type=jnp.float32).astype(
        jnp.bfloat16
    )
    outbound = jnp.broadcast_to(outbound[:, None], (EXPERTS, group_size, CAP, model_width))
    outbound = outbound.reshape(devices, CAP, model_width)
    arrived = lax.all_to_all(outbound, EP_TP, split_axis=0, concat_axis=0, tiled=True)
    partial_value = expert_rows(
        arrived.reshape(-1, model_width), expert_gate, expert_up, expert_down
    )
    returned = lax.all_to_all(
        partial_value.reshape(arrived.shape).astype(jnp.bfloat16),
        EP_TP,
        split_axis=0,
        concat_axis=0,
        tiled=True,
    ).astype(jnp.float32)
    summed = jnp.sum(returned.reshape(EXPERTS, group_size, CAP, model_width), axis=1)
    combine_weights = matches * weights.reshape(assign)[:, None, None]
    token_weights = jnp.einsum("aec,sa->sec", combine_weights, owners)
    routed = jnp.einsum("sec,ecd->sd", token_weights, summed)
    layer_out = (after_attention + routed).astype(jnp.bfloat16)
    return (layer_out, new_latent, new_rope)


def solution(mesh):
    torus = Mesh(mesh.devices.reshape(4, 4, 4, mesh.shape["tp"]), ("ep_0", "ep_1", "ep_2", "tp"))
    placed = (
        P(EP_TP, None),
        P(EP_TP),
        P(EP_TP, None, None),
        P(EP_TP, None, None),
        P(EP_TP, None),
        P(EP_TP, None),
        P(),
        P(),
        P(),
        P(),
        P(EP_TP, None),
        P(EP_TP, None),
        P(),
        P(None, EP_TP),
        P(None, EP_TP),
        P(),
        P(None, EP_TP),
        P(None, EP_TP),
        P(None, EP_TP),
        P(EP_TP, None),
    )
    return jax.shard_map(
        local,
        mesh=torus,
        in_specs=placed,
        out_specs=(P(EP_TP, None), P(EP_TP, None), P(EP_TP, None)),
        check_vma=False,
    )
```

profile of v0, /device:TPU:1, one launch (start us, length us, event | category | flops | bytes accessed | tf_op | source)
XLA Modules:
  0.0 437.4 jit_solution(7753741035902536983)
XLA Ops:
  9.8 20.9 %all_to_all.75 = bf16[128,2,128]{2,1,0:T(2,128)(2,1)S(1)} all-to-all(bf16[128,2,128]{2,1,0:T(2,128)(2,1)S(1)} %reshape.366), channel_id=1, replica_groups=mesh['ep_0'=4,'ep_1'=4,'ep_2'=4,'tp'=2] {'ep_0','ep_1','ep_2','tp'}, dimensions={0} | all-to-all | bytes 131072 | tf_op jit(solution)/shard_map/all_to_all | solution.py:161
  36.1 6.5 %copy.77 = f32[1024,1536]{1,0:T(8,128)} copy(f32[1024,1536]{0,1:T(8,128)} %pad_maximum_fusion) | data formatting | bytes 12582912 | tf_op jit(solution)/shard_map/concatenate | solution.py:164
  45.9 10.4 %all_to_all.76 = f32[2,64,8,1536]{3,2,1,0:T(8,128)} all-to-all(f32[2,64,8,1536]{3,2,1,0:T(8,128)S(1)} %copy.78), channel_id=1, replica_groups=mesh['ep_0'=4,'ep_1'=4,'ep_2'=4,'tp'=2] {'tp'}, dimensions={0} | all-to-all | bytes 12582912 | tf_op jit(solution)/shard_map/all_to_all | solution.py:24
  56.2 5.4 %reduce_sum.91 = f32[64,8,1536]{2,1,0:T(8,128)} reduce(f32[2,64,8,1536]{3,2,1,0:T(8,128)} %all_to_all.76, f32[]{:T(128)} %constant.38.clone.1), dimensions={0}, to_apply=%region_1.0 | reduce | flops 786432 | bytes 9437188 | tf_op jit(solution)/shard_map/reduce_sum | solution.py:25
  61.6 46.3 %all_to_all.77 = f32[64,8,1536]{2,1,0:T(8,128)} all-to-all(f32[64,8,1536]{2,1,0:T(8,128)} %reduce_sum.91), channel_id=1, replica_groups=mesh['ep_0'=4,'ep_1'=4,'ep_2'=4,'tp'=2] {'ep_0','ep_1','ep_2'}, dimensions={0} | all-to-all | bytes 6291456 | tf_op jit(solution)/shard_map/all_to_all | solution.py:32
  111.4 5.7 %all-to-all-start.3 = ((bf16[64,8,1024]{2,1,0:T(8,128)(2,1)}), bf16[64,8,1024]{2,1,0:T(8,128)(2,1)S(1)}, u32[]{:S(2)}, u32[]{:S(2)}) async-start(bf16[64,8,1024]{2,1,0:T(8,128)(2,1)} %broadcast_in_dim.15), calls=%async_computation.3 | async-start | bytes 2097152 | tf_op jit(solution)/shard_map/all_to_all | solution.py:38
  117.8 17.4 %all-to-all-done.3 = bf16[64,8,1024]{2,1,0:T(8,128)(2,1)S(1)} async-done(((bf16[64,8,1024]{2,1,0:T(8,128)(2,1)}), bf16[64,8,1024]{2,1,0:T(8,128)(2,1)S(1)}, u32[]{:S(2)}, u32[]{:S(2)}) %all-to-all-start.3) | async-done | bytes 1048608 | tf_op jit(solution)/shard_map/all_to_all | solution.py:38
  136.0 6.9 %all_to_all.78 = bf16[2,64,8,1024]{3,1,2,0:T(8,128)(2,1)S(1)} all-to-all(bf16[2,64,8,1024]{3,1,2,0:T(8,128)(2,1)S(1)} %broadcast_in_dim.16), channel_id=1, replica_groups=mesh['ep_0'=4,'ep_1'=4,'ep_2'=4,'tp'=2] {'tp'}, dimensions={0} | all-to-all | bytes 4194304 | tf_op jit(solution)/shard_map/all_to_all | solution.py:38
  155.9 13.6 %all-to-all-done.5 = bf16[128,8,144]{2,1,0:T(8,128)(2,1)S(1)} async-done(((bf16[128,8,144]{2,1,0:T(8,128)(2,1)}), bf16[128,8,144]{2,1,0:T(8,128)(2,1)S(1)}, u32[]{:S(2)}, u32[]{:S(2)}) %all-to-all-start.5) | async-done | bytes 294944 | tf_op jit(solution)/shard_map/all_to_all | solution.py:189
  170.8 5.9 %fusion.83 = f32[8,32,1024]{2,1,0:T(8,128)S(1)} fusion(bf16[8,32,512]{2,1,0:T(8,128)(2,1)S(1)} %reshape.347, bf16[8,1024,512]{2,1,0:T(8,128)(2,1)} %param.22), kind=kOutput, calls=%fused_computation.115 | convolution fusion | flops 268435456 | bytes 9699328 | tf_op jit(solution)/shard_map/shl,spl->shp/dot_general | solution.py:109
  177.9 5.2 %fusion.7 = bf16[8,32,512]{2,1,0:T(8,128)(2,1)S(1)} fusion(bf16[8,1024,512]{2,1,0:T(8,128)(2,1)} %param.22, f32[8,32,1024]{2,1,0:T(8,128)S(1)} %get-tuple-element.14, f32[8,32]{1,0:T(8,128)S(1)} %get-tuple-element.8, f32[8,32]{1,0:T(8,128)S(1)} %fusion.72, f32[8,512]{1,0:T(8,128)S(1)} %get-tuple-element.3, f32[8,32]{1,0:T(8,128)S(1)} %get-tuple-element.7), kind=kOutput, calls=%fused_computation.15 | convolution fusion | flops 269615104 | bytes 9718784 | tf_op jit(solution)/shard_map/shp,spl->shl/dot_general | solution.py:124
  183.1 5.2 %fusion.11 = bf16[8,4096]{1,0:T(8,128)(2,1)} fusion(bf16[512,32,128]{2,1,0:T(8,128)(2,1)S(1)} %copy-done.2, bf16[8,32,512]{2,1,0:T(8,128)(2,1)S(1)} %fusion.7), kind=kOutput, calls=%fused_computation.18 | convolution fusion | flops 33587200 | bytes 4521984 | tf_op jit(solution)/shard_map/shl,lhv->shv/dot_general | solution.py:198
  188.9 66.1 %all-gather.2.cloned.1.call-done = bf16[1024,4096]{1,0:T(8,128)(2,1)} async-done(((bf16[8,4096]{1,0:T(8,128)(2,1)}), bf16[1024,4096]{1,0:T(8,128)(2,1)}) %all-gather.2.cloned.1.call-update) | async-done | bytes 8388624 | tf_op jit(solution)/shard_map/all_gather | solution.py:201
  254.9 5.9 %convolution_convert_fusion.3 = bf16[1024,32]{0,1:T(8,128)(2,1)S(1)} fusion(bf16[1024,4096]{1,0:T(8,128)(2,1)} %all-gather.2.cloned.1.call-done, bf16[4096,32]{0,1:T(8,128)(2,1)S(1)} %copy-done.6), kind=kOutput, calls=%fused_computation.19 | convolution fusion | flops 268468224 | bytes 8716288 | tf_op jit(solution)/shard_map/dot_general | solution.py:200
  261.9 5.4 %all-to-all-start.6 = ((bf16[128,2,128]{2,1,0:T(2,128)(2,1)}), bf16[128,2,128]{2,1,0:T(2,128)(2,1)S(1)}, u32[]{:S(2)}, u32[]{:S(2)}) async-start(bf16[128,2,128]{2,1,0:T(2,128)(2,1)} %reshape.368), calls=%async_computation.6 | async-start | bytes 131072 | tf_op jit(solution)/shard_map/all_to_all | solution.py:205
  267.3 9.5 %all-to-all-done.6 = bf16[128,2,128]{2,1,0:T(2,128)(2,1)S(1)} async-done(((bf16[128,2,128]{2,1,0:T(2,128)(2,1)}), bf16[128,2,128]{2,1,0:T(2,128)(2,1)S(1)}, u32[]{:S(2)}, u32[]{:S(2)}) %all-to-all-start.6) | async-done | bytes 65568 | tf_op jit(solution)/shard_map/all_to_all | solution.py:205
  280.2 57.3 %all_to_all.79 = bf16[128,3,4096]{2,1,0:T(4,128)(2,1)} all-to-all(bf16[128,3,4096]{2,1,0:T(4,128)(2,1)S(1)} %bitcast.84), channel_id=1, replica_groups=mesh['ep_0'=4,'ep_1'=4,'ep_2'=4,'tp'=2] {'ep_0','ep_1','ep_2','tp'}, dimensions={0} | all-to-all | bytes 6291456 | tf_op jit(solution)/shard_map/all_to_all | solution.py:219
  337.5 7.4 %reshape.350 = bf16[384,4096]{1,0:T(8,128)(2,1)} reshape(bf16[128,3,4096]{2,1,0:T(4,128)(2,1)} %all_to_all.79) | data formatting | bytes 6291456 | tf_op jit(solution)/shard_map/reshape | solution.py:221
  344.9 5.1 %fusion.85 = f32[384,448]{0,1:T(8,128)S(1)} fusion(bf16[384,4096]{1,0:T(8,128)(2,1)} %reshape.350, bf16[4096,448]{0,1:T(8,128)(2,1)} %param.37), kind=kOutput, calls=%fused_computation.117 | convolution fusion | flops 1409286144 | bytes 7503872 | tf_op jit(solution)/shard_map/dot_general | solution.py:98
  350.0 9.6 %convolution_convert_fusion = bf16[384,4096]{1,0:T(8,128)(2,1)} fusion(bf16[448,4096]{1,0:T(8,128)(2,1)} %param.39, bf16[384,4096]{1,0:T(8,128)(2,1)} %reshape.350, bf16[4096,448]{0,1:T(8,128)(2,1)} %param.38, f32[384,448]{0,1:T(8,128)S(1)} %fusion.85), kind=kOutput, calls=%fused_computation.2 | convolution fusion | flops 2821177344 | bytes 14319616 | tf_op jit(solution)/shard_map/dot_general | solution.py:101
  359.6 7.1 %convert_element_type.144 = bf16[128,3,4096]{2,1,0:T(4,128)(2,1)} reshape(bf16[384,4096]{1,0:T(8,128)(2,1)} %convolution_convert_fusion) | data formatting | bytes 6291456 | tf_op jit(solution)/shard_map/convert_element_type | solution.py:224
  366.7 5.6 %all-to-all-start.8 = ((bf16[128,3,4096]{2,1,0:T(4,128)(2,1)}), bf16[128,3,4096]{2,1,0:T(4,128)(2,1)}, u32[]{:S(2)}, u32[]{:S(2)}) async-start(bf16[128,3,4096]{2,1,0:T(4,128)(2,1)} %convert_element_type.144), calls=%async_computation.8 | async-start | bytes 8388608 | tf_op jit(solution)/shard_map/all_to_all | solution.py:223
  373.3 51.8 %all-to-all-done.8 = bf16[128,3,4096]{2,1,0:T(4,128)(2,1)} async-done(((bf16[128,3,4096]{2,1,0:T(4,128)(2,1)}), bf16[128,3,4096]{2,1,0:T(4,128)(2,1)}, u32[]{:S(2)}, u32[]{:S(2)}) %all-to-all-start.8) | async-done | bytes 3145760 | tf_op jit(solution)/shard_map/all_to_all | solution.py:223
  425.1 4.4 %convert_reduce_fusion = bf16[8,3,4096]{2,1,0:T(4,128)(2,1)S(1)} fusion(bf16[128,3,4096]{2,1,0:T(4,128)(2,1)} %all-to-all-done.8), kind=kLoop, calls=%fused_computation | loop fusion | flops 3047424 | bytes 3342336 | tf_op jit(solution)/shard_map/reduce_sum | solution.py:230
  (109 shorter events, 38.2 us)
Async XLA Ops:
  7.2 169.9 %copy-start = (bf16[8,1024,64]{1,2,0:T(8,128)(2,1)S(1)}, bf16[8,1024,64]{1,2,0:T(8,128)(2,1)}, u32[]{:S(2)}) copy-start(bf16[8,1024,64]{1,2,0:T(8,128)(2,1)} %param.23) | copy-start | bytes 3145732
  7.2 24.9 %copy-start.7 = (bf16[32,1024]{1,0:T(8,128)(2,1)S(1)}, bf16[32,1024]{1,0:T(8,128)(2,1)}, u32[]{:S(2)}) copy-start(bf16[32,1024]{1,0:T(8,128)(2,1)} %param.30) | copy-start | bytes 196612
  61.6 48.6 %copy-start.11 = (f32[1024]{0:T(1024)S(1)}, f32[1024]{0:T(1024)}, u32[]{:S(2)}) copy-start(f32[1024]{0:T(1024)} %param.28) | copy-start | bytes 12292
  107.9 9.2 %copy-start.14 = (s32[8]{0:T(128)S(1)}, s32[8]{0:T(128)}, u32[]{:S(2)}) copy-start(s32[8]{0:T(128)} %param.21) | copy-start | bytes 100
  108.0 9.2 %copy-start.4 = (bf16[4096,64]{0,1:T(8,128)(2,1)S(1)}, bf16[4096,64]{0,1:T(8,128)(2,1)}, u32[]{:S(2)}) copy-start(bf16[4096,64]{0,1:T(8,128)(2,1)} %param.32) | copy-start | bytes 1572868
  111.4 23.8 %all-to-all-start.3 = ((bf16[64,8,1024]{2,1,0:T(8,128)(2,1)}), bf16[64,8,1024]{2,1,0:T(8,128)(2,1)S(1)}, u32[]{:S(2)}, u32[]{:S(2)}) async-start(bf16[64,8,1024]{2,1,0:T(8,128)(2,1)} %broadcast_in_dim.15), calls=%async_computation.3 | async-start | bytes 2097152 | tf_op jit(solution)/shard_map/all_to_all | solution.py:38
  142.9 6.3 %copy-start.8 = (bf16[1024,16]{0,1:T(8,128)(2,1)S(1)}, bf16[1024,16]{0,1:T(8,128)(2,1)}, u32[]{:S(2)}) copy-start(bf16[1024,16]{0,1:T(8,128)(2,1)} %param.34) | copy-start | bytes 98308
  146.4 3.5 copy-start.5
  149.2 6.5 %copy-start.12 = (f32[512]{0:T(512)S(1)}, f32[512]{0:T(512)}, u32[]{:S(2)}) copy-start(f32[512]{0:T(512)} %param.29) | copy-start | bytes 6148
  152.0 17.5 %all-to-all-start.5 = ((bf16[128,8,144]{2,1,0:T(8,128)(2,1)}), bf16[128,8,144]{2,1,0:T(8,128)(2,1)S(1)}, u32[]{:S(2)}, u32[]{:S(2)}) async-start(bf16[128,8,144]{2,1,0:T(8,128)(2,1)} %copy.82), calls=%async_computation.5 | async-start | bytes 1048576 | tf_op jit(solution)/shard_map/all_to_all | solution.py:189
  155.7 99.2 %all-gather.2.cloned.1.call-start = ((), (), s32[]{:S(2)}) async-start(), calls=%async_computation.9 | async-start | bytes 8454144 | tf_op jit(solution)/shard_map/all_gather | solution.py:201
  155.8 20.9 %copy-start.10 = (bf16[8,512]{1,0:T(8,128)(2,1)}, bf16[8,512]{1,0:T(8,128)(2,1)S(1)}, u32[]{:S(2)}) copy-start(bf16[8,512]{1,0:T(8,128)(2,1)S(1)} %get-tuple-element.4) | copy-start | bytes 24580
  177.9 5.2 %copy-start.2 = (bf16[512,32,128]{2,1,0:T(8,128)(2,1)S(1)}, bf16[512,32,128]{2,1,0:T(8,128)(2,1)}, u32[]{:S(2)}) copy-start(bf16[512,32,128]{2,1,0:T(8,128)(2,1)} %param.35) | copy-start | bytes 12582916
  183.1 5.3 %copy-start.13 = (s32[8,2]{0,1:T(2,128)S(1)}, s32[8,2]{0,1:T(2,128)}, u32[]{:S(2)}) copy-start(s32[8,2]{0,1:T(2,128)} %param.24) | copy-start | bytes 196
  183.1 71.8 %copy-start.6 = (bf16[4096,32]{0,1:T(8,128)(2,1)S(1)}, bf16[4096,32]{0,1:T(8,128)(2,1)}, u32[]{:S(2)}) copy-start(bf16[4096,32]{0,1:T(8,128)(2,1)} %param.36) | copy-start | bytes 786436
  188.9 88.5 %copy-start.3 = (bf16[8,4096]{1,0:T(8,128)(2,1)S(1)}, bf16[8,4096]{1,0:T(8,128)(2,1)}, u32[]{:S(2)}) copy-start(bf16[8,4096]{1,0:T(8,128)(2,1)} %param.20) | copy-start | bytes 196612
  260.9 16.7 %copy-start.9 = (f32[4096]{0:T(1024)S(1)}, f32[4096]{0:T(1024)}, u32[]{:S(2)}) copy-start(f32[4096]{0:T(1024)} %param.27) | copy-start | bytes 49156
  261.9 14.9 %all-to-all-start.6 = ((bf16[128,2,128]{2,1,0:T(2,128)(2,1)}), bf16[128,2,128]{2,1,0:T(2,128)(2,1)S(1)}, u32[]{:S(2)}, u32[]{:S(2)}) async-start(bf16[128,2,128]{2,1,0:T(2,128)(2,1)} %reshape.368), calls=%async_computation.6 | async-start | bytes 131072 | tf_op jit(solution)/shard_map/all_to_all | solution.py:205
  366.7 5.7 %copy-start.15 = (bf16[8,2]{0,1:T(2,128)(2,1)S(1)}, bf16[8,2]{0,1:T(2,128)(2,1)}, u32[]{:S(2)}) copy-start(bf16[8,2]{0,1:T(2,128)(2,1)} %param.25) | copy-start | bytes 100
  366.7 58.4 %all-to-all-start.8 = ((bf16[128,3,4096]{2,1,0:T(4,128)(2,1)}), bf16[128,3,4096]{2,1,0:T(4,128)(2,1)}, u32[]{:S(2)}, u32[]{:S(2)}) async-start(bf16[128,3,4096]{2,1,0:T(4,128)(2,1)} %convert_element_type.144), calls=%async_computation.8 | async-start | bytes 8388608 | tf_op jit(solution)/shard_map/all_to_all | solution.py:223
  372.4 58.2 %copy-start.1 = (bf16[8,1024,64]{1,2,0:T(8,128)(2,1)S(1)}, bf16[8,1024,64]{1,2,0:T(8,128)(2,1)}, u32[]{:S(2)}) copy-start(bf16[8,1024,64]{1,2,0:T(8,128)(2,1)} %param.23) | copy-start | bytes 3145732
Sparse Core Ops, SparseCore 0:
  188.5 66.3 all-gather.1
where the time goes:
time: 439 us; the launch traced here: 437 us
  waiting for transfers between devices  158 us (36%)
  blocking collectives  142 us (32%)
  matrix products  42.9 us (10%)
  local copies, waits for them, and re-layouts  39.7 us (9%)
  starting transfers between devices  20.5 us (5%)
  other arithmetic  19.6 us (4%)
  between operations  14.5 us (3%)
    all_gather x1, waiting for transfers between devices, local(): lax.all_gather(values, EP_TP, axis=0, tiled=True)  66.1 us
    all_to_all x1, blocking collectives, local(): lax.all_to_all(outbound, EP_TP, split_axis=0, concat_axis=0, tiled=True)  57.3 us
    all_to_all x1, waiting for transfers between devices, local(): lax.all_to_all(partial_value.reshape(arrived.shape).astype(jnp.bfloat16),...  51.8 us
    all_to_all x1, blocking collectives, sum_by_axis(): lax.all_to_all(nearer, far, split_axis=0, concat_axis=0, tiled=True)  46.3 us
    all_to_all x1, blocking collectives, local(): lax.all_to_all(normed, EP_TP, split_axis=1, concat_axis=0, tiled=True)  20.9 us
    all_to_all x1, waiting for transfers between devices, sent_to_all(): lax.all_to_all(jnp.broadcast_to(shard[None], (peers, *shard.shape)), axis...  17.4 us
    all_to_all x1, waiting for transfers between devices, local(): lax.all_to_all(columns, EP_TP, split_axis=0, concat_axis=1, tiled=True)  13.6 us
    all_to_all x1, blocking collectives, sent_and_summed(): lax.all_to_all(parts, axis, split_axis=0, concat_axis=0, tiled=True)  10.4 us
  transfers between devices with their start and end apart: 5, of which 5 were waited for; matrix products, arithmetic and copies ran while one was open for 0% of the time, Pallas kernels for 0%

commit v1 on v0

--- a/solution.py
+++ b/solution.py
@@ -12,6 +12,11 @@
 EP_TP = ("ep_0", "ep_1", "ep_2", "tp")
 epsilon = 1e-06
 rope_base = 10000.0
+
+
+def swapped_in(x, mesh_axis, along):
+    sent = jnp.stack([x] * lax.axis_size(mesh_axis))
+    return jnp.concatenate(lax.all_to_all(sent, mesh_axis, 0, 0), axis=along)
 
 
 def cut_along(shard, dim, peers):
@@ -198,9 +203,7 @@
     values = jnp.einsum("shl,lhv->shv", mixture, value_up, preferred_element_type=jnp.float32)
     values = values.astype(jnp.bfloat16).reshape(sequences, -1)
     output_cols = jnp.dot(
-        lax.all_gather(values, EP_TP, axis=0, tiled=True),
-        output_weight,
-        preferred_element_type=jnp.float32,
+        swapped_in(values, EP_TP, 0), output_weight, preferred_element_type=jnp.float32
     ).astype(jnp.bfloat16)
     attended = lax.all_to_all(output_cols, EP_TP, split_axis=0, concat_axis=1, tiled=True)
     after_attention = stream + attended.astype(jnp.float32)

time: 439 us -> 492 us (1.12); the launches traced: 437 us -> 484 us
  waiting for transfers between devices: 158 us -> 191 us
  between operations: 14.5 us -> 1.5 us
  starting transfers between devices: 20.5 us -> 32.6 us
  blocking collectives: 142 us -> 153 us
    all_to_all x0 -> x1, waiting for transfers between devices: none -> 98.7 us  [swapped_in(): return jnp.concatenate(lax.all_to_all(sent, mesh_axis, 0, 0), axis=along)]
    all_gather x1 -> x0, waiting for transfers between devices: 66.1 us -> none  [local(): lax.all_gather(values, EP_TP, axis=0, tiled=True)]
    all_to_all x1, blocking collectives: 6.9 us -> 18.3 us  [sent_to_all(): lax.all_to_all(jnp.broadcast_to(shard[None], (peers, *shard.shape)), axis...]
    all_to_all x1, starting transfers between devices: 5.36 us -> 11.8 us  [local(): lax.all_to_all(output_cols, EP_TP, split_axis=0, concat_axis=1, tiled=True)]
    all_to_all x0 -> x1, starting transfers between devices: none -> 5.75 us  [swapped_in(): return jnp.concatenate(lax.all_to_all(sent, mesh_axis, 0, 0), axis=along)]
where the time goes in v1:
time: 492 us; the launch traced here: 484 us
  waiting for transfers between devices  191 us (39%)
  blocking collectives  153 us (31%)
  local copies, waits for them, and re-layouts  43.9 us (9%)
  matrix products  42.3 us (9%)
  starting transfers between devices  32.6 us (7%)
  other arithmetic  19.6 us (4%)
    all_to_all x1, waiting for transfers between devices, swapped_in(): return jnp.concatenate(lax.all_to_all(sent, mesh_axis, 0, 0), axis=along)  98.7 us
    all_to_all x1, blocking collectives, local(): lax.all_to_all(outbound, EP_TP, split_axis=0, concat_axis=0, tiled=True)  57.3 us
    all_to_all x1, waiting for transfers between devices, local(): lax.all_to_all(partial_value.reshape(arrived.shape).astype(jnp.bfloat16),...  51.8 us
    all_to_all x1, blocking collectives, sum_by_axis(): lax.all_to_all(nearer, far, split_axis=0, concat_axis=0, tiled=True)  46.3 us
    all_to_all x1, blocking collectives, local(): lax.all_to_all(normed, EP_TP, split_axis=1, concat_axis=0, tiled=True)  20.9 us
    all_to_all x1, blocking collectives, sent_to_all(): lax.all_to_all(jnp.broadcast_to(shard[None], (peers, *shard.shape)), axis...  18.3 us
    all_to_all x1, waiting for transfers between devices, sent_to_all(): lax.all_to_all(jnp.broadcast_to(shard[None], (peers, *shard.shape)), axis...  17.4 us
    all_to_all x1, waiting for transfers between devices, local(): lax.all_to_all(columns, EP_TP, split_axis=0, concat_axis=1, tiled=True)  13.6 us
  transfers between devices with their start and end apart: 5, of which 5 were waited for; matrix products, arithmetic and copies ran while one was open for 0% of the time, Pallas kernels for 0%

profile of v1, /device:TPU:1, one launch (start us, length us, event | category | flops | bytes accessed | tf_op | source)
XLA Modules:
  0.0 484.2 jit_solution(4596341259302113633)
XLA Ops:
  3.2 20.9 %all_to_all.80 = bf16[128,2,128]{2,1,0:T(2,128)(2,1)S(1)} all-to-all(bf16[128,2,128]{2,1,0:T(2,128)(2,1)S(1)} %reshape.368), channel_id=1, replica_groups=mesh['ep_0'=4,'ep_1'=4,'ep_2'=4,'tp'=2] {'ep_0','ep_1','ep_2','tp'}, dimensions={0} | all-to-all | bytes 131072 | tf_op jit(solution)/shard_map/all_to_all | solution.py:166
  29.6 6.5 %copy.77 = f32[1024,1536]{1,0:T(8,128)} copy(f32[1024,1536]{0,1:T(8,128)} %pad_maximum_fusion) | data formatting | bytes 12582912 | tf_op jit(solution)/shard_map/concatenate | solution.py:169
  39.4 10.4 %all_to_all.81 = f32[2,64,8,1536]{3,2,1,0:T(8,128)} all-to-all(f32[2,64,8,1536]{3,2,1,0:T(8,128)S(1)} %copy.78), channel_id=1, replica_groups=mesh['ep_0'=4,'ep_1'=4,'ep_2'=4,'tp'=2] {'tp'}, dimensions={0} | all-to-all | bytes 12582912 | tf_op jit(solution)/shard_map/all_to_all | solution.py:29
  49.8 5.4 %reduce_sum.91 = f32[64,8,1536]{2,1,0:T(8,128)} reduce(f32[2,64,8,1536]{3,2,1,0:T(8,128)} %all_to_all.81, f32[]{:T(128)} %constant.38.clone.1), dimensions={0}, to_apply=%region_1.0 | reduce | flops 786432 | bytes 9437188 | tf_op jit(solution)/shard_map/reduce_sum | solution.py:30
  55.2 46.3 %all_to_all.82 = f32[64,8,1536]{2,1,0:T(8,128)} all-to-all(f32[64,8,1536]{2,1,0:T(8,128)} %reduce_sum.91), channel_id=1, replica_groups=mesh['ep_0'=4,'ep_1'=4,'ep_2'=4,'tp'=2] {'ep_0','ep_1','ep_2'}, dimensions={0} | all-to-all | bytes 6291456 | tf_op jit(solution)/shard_map/all_to_all | solution.py:37
  104.9 5.7 %all-to-all-start.3 = ((bf16[64,8,1024]{2,1,0:T(8,128)(2,1)}), bf16[64,8,1024]{2,1,0:T(8,128)(2,1)S(1)}, u32[]{:S(2)}, u32[]{:S(2)}) async-start(bf16[64,8,1024]{2,1,0:T(8,128)(2,1)} %broadcast_in_dim.15), calls=%async_computation.3 | async-start | bytes 2097152 | tf_op jit(solution)/shard_map/all_to_all | solution.py:43
  111.3 17.4 %all-to-all-done.3 = bf16[64,8,1024]{2,1,0:T(8,128)(2,1)S(1)} async-done(((bf16[64,8,1024]{2,1,0:T(8,128)(2,1)}), bf16[64,8,1024]{2,1,0:T(8,128)(2,1)S(1)}, u32[]{:S(2)}, u32[]{:S(2)}) %all-to-all-start.3) | async-done | bytes 1048608 | tf_op jit(solution)/shard_map/all_to_all | solution.py:43
  129.6 18.3 %all_to_all.83 = bf16[2,64,8,1024]{3,1,2,0:T(8,128)(2,1)S(1)} all-to-all(bf16[2,64,8,1024]{3,1,2,0:T(8,128)(2,1)S(1)} %broadcast_in_dim.16), channel_id=1, replica_groups=mesh['ep_0'=4,'ep_1'=4,'ep_2'=4,'tp'=2] {'tp'}, dimensions={0} | all-to-all | bytes 4194304 | tf_op jit(solution)/shard_map/all_to_all | solution.py:43
  160.6 13.6 %all-to-all-done.5 = bf16[128,8,144]{2,1,0:T(8,128)(2,1)S(1)} async-done(((bf16[128,8,144]{2,1,0:T(8,128)(2,1)}), bf16[128,8,144]{2,1,0:T(8,128)(2,1)S(1)}, u32[]{:S(2)}, u32[]{:S(2)}) %all-to-all-start.5) | async-done | bytes 294944 | tf_op jit(solution)/shard_map/all_to_all | solution.py:194
  175.5 5.9 %fusion.88 = f32[8,32,1024]{2,1,0:T(8,128)S(1)} fusion(bf16[8,32,512]{2,1,0:T(8,128)(2,1)S(1)} %reshape.349, bf16[8,1024,512]{2,1,0:T(8,128)(2,1)} %param.22), kind=kOutput, calls=%fused_computation.117 | convolution fusion | flops 268435456 | bytes 9699328 | tf_op jit(solution)/shard_map/shl,spl->shp/dot_general | solution.py:114
  182.7 5.2 %fusion.9 = bf16[8,32,512]{2,1,0:T(8,128)(2,1)S(1)} fusion(bf16[8,1024,512]{2,1,0:T(8,128)(2,1)} %param.22, f32[8,32,1024]{2,1,0:T(8,128)S(1)} %get-tuple-element.14, f32[8,32]{1,0:T(8,128)S(1)} %get-tuple-element.8, f32[8,32]{1,0:T(8,128)S(1)} %fusion.77, f32[8,512]{1,0:T(8,128)S(1)} %get-tuple-element.3, f32[8,32]{1,0:T(8,128)S(1)} %get-tuple-element.7), kind=kOutput, calls=%fused_computation.17 | convolution fusion | flops 269615104 | bytes 9718784 | tf_op jit(solution)/shard_map/shp,spl->shl/dot_general | solution.py:129
  187.9 4.6 fusion.13
  196.8 5.7 %all-to-all-start.6 = ((bf16[128,8,4096]{2,1,0:T(8,128)(2,1)}), bf16[128,8,4096]{2,1,0:T(8,128)(2,1)}, u32[]{:S(2)}, u32[]{:S(2)}) async-start(bf16[128,8,4096]{2,1,0:T(8,128)(2,1)} %stack.3), calls=%async_computation.6 | async-start | bytes 16777216 | tf_op jit(solution)/shard_map/all_to_all | solution.py:19
  203.0 98.7 %all-to-all-done.6 = bf16[128,8,4096]{2,1,0:T(8,128)(2,1)} async-done(((bf16[128,8,4096]{2,1,0:T(8,128)(2,1)}), bf16[128,8,4096]{2,1,0:T(8,128)(2,1)}, u32[]{:S(2)}, u32[]{:S(2)}) %all-to-all-start.6) | async-done | bytes 8388640 | tf_op jit(solution)/shard_map/all_to_all | solution.py:19
  301.8 6.0 %fusion.16 = bf16[1024,32]{0,1:T(8,128)(2,1)S(1)} fusion(bf16[4096,32]{0,1:T(8,128)(2,1)S(1)} %copy-done.6, bf16[128,8,4096]{2,1,0:T(8,128)(2,1)} %all-to-all-done.6), kind=kOutput, calls=%fused_computation.21 | convolution fusion | flops 268468224 | bytes 8716288 | tf_op jit(solution)/shard_map/dot_general | solution.py:205
  308.7 11.8 %all-to-all-start.7 = ((bf16[128,2,128]{2,1,0:T(2,128)(2,1)}), bf16[128,2,128]{2,1,0:T(2,128)(2,1)S(1)}, u32[]{:S(2)}, u32[]{:S(2)}) async-start(bf16[128,2,128]{2,1,0:T(2,128)(2,1)} %reshape.370), calls=%async_computation.7 | async-start | bytes 131072 | tf_op jit(solution)/shard_map/all_to_all | solution.py:208
  320.5 9.5 %all-to-all-done.7 = bf16[128,2,128]{2,1,0:T(2,128)(2,1)S(1)} async-done(((bf16[128,2,128]{2,1,0:T(2,128)(2,1)}), bf16[128,2,128]{2,1,0:T(2,128)(2,1)S(1)}, u32[]{:S(2)}, u32[]{:S(2)}) %all-to-all-start.7) | async-done | bytes 65568 | tf_op jit(solution)/shard_map/all_to_all | solution.py:208
  333.4 57.3 %all_to_all.84 = bf16[128,3,4096]{2,1,0:T(4,128)(2,1)} all-to-all(bf16[128,3,4096]{2,1,0:T(4,128)(2,1)S(1)} %bitcast.88), channel_id=1, replica_groups=mesh['ep_0'=4,'ep_1'=4,'ep_2'=4,'tp'=2] {'ep_0','ep_1','ep_2','tp'}, dimensions={0} | all-to-all | bytes 6291456 | tf_op jit(solution)/shard_map/all_to_all | solution.py:222
  390.8 7.4 %reshape.352 = bf16[384,4096]{1,0:T(8,128)(2,1)} reshape(bf16[128,3,4096]{2,1,0:T(4,128)(2,1)} %all_to_all.84) | data formatting | bytes 6291456 | tf_op jit(solution)/shard_map/reshape | solution.py:224
  398.2 5.1 %fusion.90 = f32[384,448]{0,1:T(8,128)S(1)} fusion(bf16[384,4096]{1,0:T(8,128)(2,1)} %reshape.352, bf16[4096,448]{0,1:T(8,128)(2,1)} %param.37), kind=kOutput, calls=%fused_computation.119 | convolution fusion | flops 1409286144 | bytes 7503872 | tf_op jit(solution)/shard_map/dot_general | solution.py:103
  403.3 9.6 %convolution_convert_fusion = bf16[384,4096]{1,0:T(8,128)(2,1)} fusion(bf16[448,4096]{1,0:T(8,128)(2,1)} %param.39, bf16[384,4096]{1,0:T(8,128)(2,1)} %reshape.352, bf16[4096,448]{0,1:T(8,128)(2,1)} %param.38, f32[384,448]{0,1:T(8,128)S(1)} %fusion.90), kind=kOutput, calls=%fused_computation.4 | convolution fusion | flops 2821177344 | bytes 14319616 | tf_op jit(solution)/shard_map/dot_general | solution.py:106
  412.9 7.1 %convert_element_type.144 = bf16[128,3,4096]{2,1,0:T(4,128)(2,1)} reshape(bf16[384,4096]{1,0:T(8,128)(2,1)} %convolution_convert_fusion) | data formatting | bytes 6291456 | tf_op jit(solution)/shard_map/convert_element_type | solution.py:227
  420.0 5.6 %all-to-all-start.9 = ((bf16[128,3,4096]{2,1,0:T(4,128)(2,1)}), bf16[128,3,4096]{2,1,0:T(4,128)(2,1)}, u32[]{:S(2)}, u32[]{:S(2)}) async-start(bf16[128,3,4096]{2,1,0:T(4,128)(2,1)} %convert_element_type.144), calls=%async_computation.9 | async-start | bytes 8388608 | tf_op jit(solution)/shard_map/all_to_all | solution.py:226
  426.6 51.8 %all-to-all-done.9 = bf16[128,3,4096]{2,1,0:T(4,128)(2,1)} async-done(((bf16[128,3,4096]{2,1,0:T(4,128)(2,1)}), bf16[128,3,4096]{2,1,0:T(4,128)(2,1)}, u32[]{:S(2)}, u32[]{:S(2)}) %all-to-all-start.9) | async-done | bytes 3145760 | tf_op jit(solution)/shard_map/all_to_all | solution.py:226
  (109 shorter events, 46.8 us)
Async XLA Ops:
  0.6 181.3 %copy-start = (bf16[8,1024,64]{1,2,0:T(8,128)(2,1)S(1)}, bf16[8,1024,64]{1,2,0:T(8,128)(2,1)}, u32[]{:S(2)}) copy-start(bf16[8,1024,64]{1,2,0:T(8,128)(2,1)} %param.23) | copy-start | bytes 3145732
  0.6 25.3 %copy-start.7 = (bf16[32,512]{1,0:T(8,128)(2,1)S(1)}, bf16[32,512]{1,0:T(8,128)(2,1)}, u32[]{:S(2)}) copy-start(bf16[32,512]{1,0:T(8,128)(2,1)} %param.31) | copy-start | bytes 98308
  55.2 48.6 %copy-start.11 = (f32[1024]{0:T(1024)S(1)}, f32[1024]{0:T(1024)}, u32[]{:S(2)}) copy-start(f32[1024]{0:T(1024)} %param.28) | copy-start | bytes 12292
  101.5 9.2 %copy-start.14 = (s32[8]{0:T(128)S(1)}, s32[8]{0:T(128)}, u32[]{:S(2)}) copy-start(s32[8]{0:T(128)} %param.21) | copy-start | bytes 100
  101.5 9.2 %copy-start.4 = (bf16[4096,64]{0,1:T(8,128)(2,1)S(1)}, bf16[4096,64]{0,1:T(8,128)(2,1)}, u32[]{:S(2)}) copy-start(bf16[4096,64]{0,1:T(8,128)(2,1)} %param.32) | copy-start | bytes 1572868
  104.9 23.8 %all-to-all-start.3 = ((bf16[64,8,1024]{2,1,0:T(8,128)(2,1)}), bf16[64,8,1024]{2,1,0:T(8,128)(2,1)S(1)}, u32[]{:S(2)}, u32[]{:S(2)}) async-start(bf16[64,8,1024]{2,1,0:T(8,128)(2,1)} %broadcast_in_dim.15), calls=%async_computation.3 | async-start | bytes 2097152 | tf_op jit(solution)/shard_map/all_to_all | solution.py:43
  147.8 6.3 %copy-start.5 = (bf16[1024,128]{1,0:T(8,128)(2,1)S(1)}, bf16[1024,128]{1,0:T(8,128)(2,1)}, u32[]{:S(2)}) copy-start(bf16[1024,128]{1,0:T(8,128)(2,1)} %param.33) | copy-start | bytes 786436
  151.3 3.6 copy-start.8
  154.1 6.4 %copy-start.12 = (f32[512]{0:T(512)S(1)}, f32[512]{0:T(512)}, u32[]{:S(2)}) copy-start(f32[512]{0:T(512)} %param.29) | copy-start | bytes 6148
  156.8 17.4 %all-to-all-start.5 = ((bf16[128,8,144]{2,1,0:T(8,128)(2,1)}), bf16[128,8,144]{2,1,0:T(8,128)(2,1)S(1)}, u32[]{:S(2)}, u32[]{:S(2)}) async-start(bf16[128,8,144]{2,1,0:T(8,128)(2,1)} %copy.82), calls=%async_computation.5 | async-start | bytes 1048576 | tf_op jit(solution)/shard_map/all_to_all | solution.py:194
  160.6 20.7 %copy-start.10 = (bf16[8,512]{1,0:T(8,128)(2,1)}, bf16[8,512]{1,0:T(8,128)(2,1)S(1)}, u32[]{:S(2)}) copy-start(bf16[8,512]{1,0:T(8,128)(2,1)S(1)} %get-tuple-element.4) | copy-start | bytes 24580
  182.7 5.2 %copy-start.2 = (bf16[512,32,128]{2,1,0:T(8,128)(2,1)S(1)}, bf16[512,32,128]{2,1,0:T(8,128)(2,1)}, u32[]{:S(2)}) copy-start(bf16[512,32,128]{2,1,0:T(8,128)(2,1)} %param.35) | copy-start | bytes 12582916
  196.8 5.8 %copy-start.13 = (s32[8,2]{0,1:T(2,128)S(1)}, s32[8,2]{0,1:T(2,128)}, u32[]{:S(2)}) copy-start(s32[8,2]{0,1:T(2,128)} %param.24) | copy-start | bytes 196
  196.8 105.0 %copy-start.6 = (bf16[4096,32]{0,1:T(8,128)(2,1)S(1)}, bf16[4096,32]{0,1:T(8,128)(2,1)}, u32[]{:S(2)}) copy-start(bf16[4096,32]{0,1:T(8,128)(2,1)} %param.36) | copy-start | bytes 786436
  196.8 105.0 %all-to-all-start.6 = ((bf16[128,8,4096]{2,1,0:T(8,128)(2,1)}), bf16[128,8,4096]{2,1,0:T(8,128)(2,1)}, u32[]{:S(2)}, u32[]{:S(2)}) async-start(bf16[128,8,4096]{2,1,0:T(8,128)(2,1)} %stack.3), calls=%async_computation.6 | async-start | bytes 16777216 | tf_op jit(solution)/shard_map/all_to_all | solution.py:19
  203.0 127.6 %copy-start.3 = (bf16[8,4096]{1,0:T(8,128)(2,1)S(1)}, bf16[8,4096]{1,0:T(8,128)(2,1)}, u32[]{:S(2)}) copy-start(bf16[8,4096]{1,0:T(8,128)(2,1)} %param.20) | copy-start | bytes 196612
  307.7 23.1 %copy-start.9 = (f32[4096]{0:T(1024)S(1)}, f32[4096]{0:T(1024)}, u32[]{:S(2)}) copy-start(f32[4096]{0:T(1024)} %param.27) | copy-start | bytes 49156
  308.7 21.4 %all-to-all-start.7 = ((bf16[128,2,128]{2,1,0:T(2,128)(2,1)}), bf16[128,2,128]{2,1,0:T(2,128)(2,1)S(1)}, u32[]{:S(2)}, u32[]{:S(2)}) async-start(bf16[128,2,128]{2,1,0:T(2,128)(2,1)} %reshape.370), calls=%async_computation.7 | async-start | bytes 131072 | tf_op jit(solution)/shard_map/all_to_all | solution.py:208
  420.0 5.7 %copy-start.15 = (bf16[8,2]{0,1:T(2,128)(2,1)S(1)}, bf16[8,2]{0,1:T(2,128)(2,1)}, u32[]{:S(2)}) copy-start(bf16[8,2]{0,1:T(2,128)(2,1)} %param.25) | copy-start | bytes 100
  420.0 58.4 %all-to-all-start.9 = ((bf16[128,3,4096]{2,1,0:T(4,128)(2,1)}), bf16[128,3,4096]{2,1,0:T(4,128)(2,1)}, u32[]{:S(2)}, u32[]{:S(2)}) async-start(bf16[128,3,4096]{2,1,0:T(4,128)(2,1)} %convert_element_type.144), calls=%async_computation.9 | async-start | bytes 8388608 | tf_op jit(solution)/shard_map/all_to_all | solution.py:226
  425.7 58.2 %copy-start.1 = (bf16[8,1024,64]{1,2,0:T(8,128)(2,1)S(1)}, bf16[8,1024,64]{1,2,0:T(8,128)(2,1)}, u32[]{:S(2)}) copy-start(bf16[8,1024,64]{1,2,0:T(8,128)(2,1)} %param.23) | copy-start | bytes 3145732
